TPU v7x, 512 devices: a whole 4x8x8 slice. The times are simulated.
512 devices in a mesh: sp: 32 (over z, x), tp: 16 (over y, core).
Axes of the slice: x: 4, y: 8, z: 8, core: 2. Of those that a mesh axis runs over, the one named last changes fastest.
Arguments:
- pool_input: bfloat16 [8192, 1024], P('sp', 'tp'), may hold values from -6 to 6
- pool_weight: bfloat16 [16, 64, 64], P('tp'), may hold values from -0.75 to 0.75
- pool_gain: bfloat16 [1024], P('tp'), may hold values from 0.099609375 to 1.8984375
- out_weight: bfloat16 [1024, 2048], P(None, 'tp'), may hold values from -0.1875 to 0.1875
- resid: bfloat16 [8192, 2048], P('sp', 'tp'), may hold values from -90 to 90
- norm_gain: bfloat16 [2048], P('tp'), may hold values from 0.099609375 to 1.8984375
- routes: int32 [8192, 2], P('sp'), may hold values from 0 to 31, all different within a row; in each aligned block of 256 rows (0 to 255, 256 to 511, ...) at most 32 rows name the same one
- route_weight: float32 [8192, 2], P('sp'), may hold values from 0.2 to 1
- expert_gate: bfloat16 [32, 2048, 4096], P('sp', None, 'tp'), may hold values from -0.375 to 0.375
- expert_up: bfloat16 [32, 2048, 4096], P('sp', None, 'tp'), may hold values from -0.375 to 0.375
- expert_down: bfloat16 [32, 4096, 2048], P('sp', 'tp'), may hold values from -0.0234375 to 0.0234375
Outputs:
- layer_out: bfloat16 [8192, 2048], P('sp', 'tp')
Inputs may be any that keep to these rules, and one draw needn't show every extreme that they name: `routes`: the 2 experts of a position differ. In each aligned block of 256 positions no expert is named by more than 32 assignments; some block reaches that bound.
All inputs are finite; a program needn't handle non-finite values.
Results may differ from a plain program's by a relative error of at most 0.0085.
Values may be sent and summed in bfloat16 or wider, within the bound.
No kernel may reach another device: no remote copies, remote signals or barrier semaphores. Data moves between devices by JAX's collectives and lax.ppermute only.
A program may use at most 64 MiB of HBM per device.

v0:
```python
import jax
import jax.numpy as jnp
from jax import lax
from jax.sharding import PartitionSpec as P

D = 2048
GSIZE = 64
REACH = 16
TOPK = 2
GATE_LIMIT = 7.0
GATE_ALPHA = 1.702
NORM_EPS = 1e-05


def from_behind(value, axis, steps):
    count = lax.axis_size(axis)
    first, last = (max(0, -steps), min(count, count - steps))
    return lax.ppermute(value, axis, [(source, source + steps) for source in range(first, last)])


def sent_to_all(value, axis):
    peers = lax.axis_size(axis)
    return lax.all_to_all(
        jnp.broadcast_to(value[None], (peers, *value.shape)), axis, 0, 0, tiled=True
    )


def taken_together(value, axis):
    everything = sent_to_all(value, axis)
    return jnp.sum(everything, axis=0)


def clamped_unit(gate_pre, up_pre):
    gate_cut = jnp.minimum(gate_pre, GATE_LIMIT)
    up_cut = jnp.clip(up_pre, -GATE_LIMIT, GATE_LIMIT)
    return (up_cut + 1.0) * gate_cut * jax.nn.sigmoid(GATE_ALPHA * gate_cut)


def window_pool(extended, width_of, position, tok_count):
    summed = jnp.zeros((tok_count, extended.shape[1]), jnp.float32)
    for offset in range(REACH):
        first_row = REACH - 1 - offset
        shifted = extended[first_row : first_row + tok_count]
        summed = summed + jnp.where(offset < width_of[None, :], shifted, 0.0)
    counted = jnp.minimum(position[:, None] + 1, width_of[None, :]).astype(jnp.float32)
    current = extended[REACH - 1 :]
    return (summed / counted - current).astype(jnp.bfloat16)


def slot_of(route_block, expert_count, capacity):
    flattened = route_block.reshape(-1)
    onehot = (flattened[:, None] == jnp.arange(expert_count, dtype=jnp.int32)[None, :]).astype(
        jnp.int32
    )
    earlier = jnp.cumsum(onehot, axis=0) - onehot
    ranked = jnp.sum(earlier * onehot, axis=1)
    return flattened * capacity + ranked


def on_device(
    pool_input,
    pool_weight,
    pool_gain,
    out_weight,
    resid,
    norm_gain,
    routes,
    route_weight,
    expert_gate,
    expert_up,
    expert_down,
):
    tok_rows, channels = pool_input.shape
    groups = pool_weight.shape[0]
    features = out_weight.shape[1]
    experts_all = lax.axis_size("sp") * expert_gate.shape[0]
    capacity = 2 * tok_rows * TOPK // experts_all
    tail_rows = pool_input[tok_rows - (REACH - 1) :]
    before = from_behind(tail_rows, "sp", 1)
    extended = jnp.concatenate([before, pool_input], axis=0).astype(jnp.float32)
    first_group = lax.axis_index("tp") * groups
    width_of = 2 ** (1 + (first_group + jnp.arange(channels, dtype=jnp.int32) // GSIZE) % 4)
    position = lax.axis_index("sp") * tok_rows + jnp.arange(tok_rows, dtype=jnp.int32)
    pooled = window_pool(extended, width_of, position, tok_rows)
    grouped = jnp.einsum(
        "tgc,gcd->tgd",
        pooled.reshape(tok_rows, groups, GSIZE),
        pool_weight,
        preferred_element_type=jnp.float32,
    )
    mixed_out = (
        (grouped * pool_gain.astype(jnp.float32).reshape(groups, GSIZE))
        .astype(jnp.bfloat16)
        .reshape(tok_rows, channels)
    )
    projected = jnp.dot(
        lax.all_gather(mixed_out, "tp", axis=1, tiled=True),
        out_weight,
        preferred_element_type=jnp.float32,
    )
    stored = lax.optimization_barrier((resid.astype(jnp.float32) + projected).astype(jnp.bfloat16))
    stream = stored.astype(jnp.float32)
    squares = taken_together(jnp.sum(stream * stream, axis=1), "tp")
    scale_row = lax.rsqrt(squares / D + NORM_EPS)
    normed_part = (stream * scale_row[:, None] * norm_gain.astype(jnp.float32)).astype(jnp.bfloat16)
    slot_index = slot_of(routes, experts_all, capacity)
    token_ids = jnp.repeat(jnp.arange(tok_rows, dtype=jnp.int32), TOPK)
    slot_token = (
        jnp.full((experts_all * capacity,), tok_rows, jnp.int32).at[slot_index].set(token_ids)
    )
    sent_rows = jnp.take(normed_part, slot_token, axis=0, mode="fill", fill_value=0).reshape(
        experts_all, capacity, features
    )
    gathered = lax.all_gather(
        lax.all_to_all(sent_rows, "sp", split_axis=0, concat_axis=0, tiled=True),
        "tp",
        axis=2,
        tiled=True,
    )
    sources = gathered.shape[0]
    slot_count = gathered.shape[1]
    flattened = gathered.reshape(sources * slot_count, gathered.shape[2])
    gate_pre = jnp.dot(flattened, expert_gate[0], preferred_element_type=jnp.float32)
    up_pre = jnp.dot(flattened, expert_up[0], preferred_element_type=jnp.float32)
    hidden = clamped_unit(gate_pre, up_pre).astype(jnp.bfloat16)
    down_piece = expert_down[0]
    summed = lax.psum_scatter(
        lax.dot_general(
            down_piece, hidden, (((0,), (1,)), ((), ())), preferred_element_type=jnp.float32
        ).astype(jnp.bfloat16),
        "tp",
        scatter_dimension=0,
        tiled=True,
    ).astype(jnp.float32)
    result = summed.astype(jnp.bfloat16).reshape(summed.shape[0], sources, slot_count)
    returned = lax.all_to_all(result, "sp", split_axis=1, concat_axis=1, tiled=True)
    flat_back = returned.reshape(returned.shape[0], experts_all * capacity)
    picked = (
        jnp.take(flat_back, slot_index, axis=1)
        .astype(jnp.float32)
        .reshape(flat_back.shape[0], tok_rows, TOPK)
    )
    combined = jnp.sum(picked * route_weight[None, :, :], axis=2)
    return (stream + combined.T).astype(jnp.bfloat16)


def solution(mesh):
    in_specs = (
        P("sp", "tp"),
        P("tp", None, None),
        P("tp"),
        P(None, "tp"),
        P("sp", "tp"),
        P("tp"),
        P("sp", None),
        P("sp", None),
        P("sp", None, "tp"),
        P("sp", None, "tp"),
        P("sp", "tp", None),
    )
    out_specs = P("sp", "tp")
    return jax.shard_map(
        on_device, mesh=mesh, in_specs=in_specs, out_specs=out_specs, check_vma=False
    )
```

profile of v0, /device:TPU:25, one launch (start us, length us, event | category | flops | bytes accessed | tf_op | source)
XLA Modules:
  0.0 242.8 jit_solution(6143387055872761771)
XLA Ops:
  6.5 0.0 copy-start
  6.5 0.0 copy-start.5
  6.5 0.9 slice.58
  7.4 3.1 %collective-permute-start = (bf16[15,64]{0,1:T(8,128)(2,1)S(1)}, bf16[15,64]{0,1:T(8,128)(2,1)S(1)}, u32[]{:S(2)}, u32[]{:S(2)}) collective-permute-start(bf16[15,64]{0,1:T(8,128)(2,1)S(1)} %slice.58), channel_id=1, source_target_pairs={{0,16},{16,32},{32,48},{48,64},{64,80},{80,96},{96,112},{112,128},... | collective-permute-start | bytes 5768 | tf_op jit(solution)/shard_map/ppermute | solution.py:18
  10.8 0.8 copy.35
  11.6 0.0 copy-start.3
  11.6 0.1 eq.28
  11.7 0.1 reshape.237
  11.9 0.7 broadcast_multiply_fusion
  12.6 1.2 reduce-window.6
  13.8 0.2 slice_reduce_fusion
  14.0 0.1 copy.40
  14.2 0.1 mul.320
  14.4 0.1 reshape.263
  14.5 0.1 fusion.28
  14.6 2.4 %scatter_custom_fusion = s32[1024]{0:T(1024)S(1)} fusion(s32[512]{0:T(512)S(1)} %bitcast.68, s32[512]{0:T(512)S(1)} %reshape.263, s32[]{:T(128)} %constant.149.clone.1), kind=kCustom, calls=%fused_computation.92 | custom fusion | bytes 4100 | tf_op jit(solution)/shard_map/scatter | solution.py:109
  17.1 0.7 convert_element_type.62
  17.8 0.0 collective-permute-done
  17.8 0.8 maximum_convert_fusion
  18.6 1.3 fusion.7
  20.0 17.9 %all-gather = bf16[256,1,1024]{0,2,1:T(8,128)(2,1)S(1)} all-gather(bf16[256,1,64]{0,2,1:T(8,128)(2,1)S(1)} %fusion.7), channel_id=2, replica_groups=mesh['sp'=32,'tp'=16] {'tp'}, dimensions={2}, use_global_device_ids=true | all-gather | bytes 557056 | tf_op jit(solution)/shard_map/all_gather | solution.py:97
  37.9 1.3 fusion.4
  39.2 0.1 fusion.22
  39.3 0.6 broadcast_in_dim.187
  39.9 6.2 %all-to-all-start = ((f32[16,1,256]{2,1,0:T(1,128)}), f32[16,1,256]{2,1,0:T(1,128)S(1)}, u32[]{:S(2)}, u32[]{:S(2)}) async-start(f32[16,1,256]{2,1,0:T(1,128)} %broadcast_in_dim.187), calls=%async_computation | async-start | bytes 32768 | tf_op jit(solution)/shard_map/all_to_all | solution.py:23
  46.1 0.0 all-gather.3.cloned.1.call-start
  46.2 0.0 copy-done.5
  46.2 0.1 broadcast_in_dim.185
  46.3 4.4 %all-to-all-done = f32[16,1,256]{2,1,0:T(1,128)S(1)} async-done(((f32[16,1,256]{2,1,0:T(1,128)}), f32[16,1,256]{2,1,0:T(1,128)S(1)}, u32[]{:S(2)}, u32[]{:S(2)}) %all-to-all-start) | async-done | bytes 16416 | tf_op jit(solution)/shard_map/all_to_all | solution.py:23
  50.7 0.1 fusion.24
  50.8 3.2 %gather_fusion = bf16[1024,128]{1,0:T(8,128)(2,1)S(1)} fusion(bf16[256,128]{1,0:T(8,128)(2,1)S(1)} %fusion.24, s32[1024]{0:T(1024)S(1)} %fusion.50), kind=kCustom, calls=%fused_computation | custom fusion | bytes 528384 | tf_op jit(solution)/shard_map/jit(_take)/gather | solution.py:111
  54.0 0.2 broadcast_select_fusion
  54.2 0.0 copy-start.4
  54.2 24.2 %all_to_all.16 = bf16[32,32,128]{2,1,0:T(8,128)(2,1)} all-to-all(bf16[32,32,128]{2,1,0:T(8,128)(2,1)S(1)} %broadcast_select_fusion), channel_id=1, replica_groups=mesh['sp'=32,'tp'=16] {'sp'}, dimensions={0} | all-to-all | bytes 524288 | tf_op jit(solution)/shard_map/all_to_all | solution.py:115
  78.4 0.0 all-gather.3.cloned.1.call-update
  78.4 0.0 reduce-scatter.4.cloned.1.call-start
  78.5 45.3 %all-gather.3.cloned.1.call-done = bf16[32,32,2048]{2,1,0:T(8,128)(2,1)} async-done(((bf16[32,32,128]{2,1,0:T(8,128)(2,1)}), bf16[32,32,2048]{2,1,0:T(8,128)(2,1)}) %all-gather.3.cloned.1.call-update) | async-done | bytes 4194320 | tf_op jit(solution)/shard_map/all_gather | solution.py:114
  123.7 0.0 copy-done.3
  123.7 4.5 %convolution_minimum_fusion = f32[1024,256]{1,0:T(8,128)} fusion(bf16[1024,2048]{1,0:T(8,128)(2,1)} %bitcast.70, bf16[1,2048,256]{2,1,0:T(8,128)(2,1)S(1)} %copy-done.3), kind=kOutput, calls=%fused_computation.4 | convolution fusion | flops 1074003968 | bytes 6291456 | tf_op jit(solution)/shard_map/dot_general | solution.py:123
  128.3 0.0 copy-done
  128.3 0.0 copy-done.4
  128.3 8.8 %convert_bitcast_fusion = bf16[2048,1024]{0,1:T(8,128)(2,1)} fusion(f32[1024,256]{1,0:T(8,128)} %convolution_minimum_fusion, bf16[1024,2048]{1,0:T(8,128)(2,1)} %bitcast.71, bf16[1,256,2048]{2,1,0:T(8,128)(2,1)S(1)} %copy-done, bf16[1,2048,256]{2,1,0:T(8,128)(2,1)S(1)} %copy-done.4), kind=kOutput, calls=%fused_computation.3 | convolution fusion | flops 2151940096 | bytes 11534336 | tf_op jit(solution)/shard_map/dot_general | solution.py:128
  137.1 6.4 %copy.43 = bf16[2048,1024]{1,0:T(8,128)(2,1)} copy(bf16[2048,1024]{0,1:T(8,128)(2,1)} %convert_bitcast_fusion) | data formatting | bytes 8388608
  143.5 0.0 copy-start.1
  143.5 0.0 copy-start.2
  143.5 0.0 reduce-scatter.4.cloned.1.call-update
  143.5 66.1 %reduce-scatter.4.cloned.1.call-done = bf16[128,1024]{1,0:T(8,128)(2,1)} async-done(((bf16[2048,1024]{1,0:T(8,128)(2,1)}), bf16[128,1024]{1,0:T(8,128)(2,1)}) %reduce-scatter.4.cloned.1.call-update) | async-done | bytes 262160
  209.6 1.8 copy.44
  211.4 9.9 %all-to-all-start.2 = ((bf16[128,32,32]{0,2,1:T(8,128)(2,1)}), bf16[128,32,32]{0,2,1:T(8,128)(2,1)S(1)}, u32[]{:S(2)}, u32[]{:S(2)}) async-start(bf16[128,32,32]{0,2,1:T(8,128)(2,1)} %bitcast.14), calls=%async_computation.2 | async-start | bytes 524288 | tf_op jit(solution)/shard_map/all_to_all | solution.py:136
  221.3 0.1 reduce_sum.41
  221.5 0.1 copy.38
  221.6 0.0 copy-done.1
  221.6 0.2 copy.39
  221.8 0.0 copy-done.2
  221.8 0.1 copy.42
  221.9 10.5 %all-to-all-done.2 = bf16[128,32,32]{0,2,1:T(8,128)(2,1)S(1)} async-done(((bf16[128,32,32]{0,2,1:T(8,128)(2,1)}), bf16[128,32,32]{0,2,1:T(8,128)(2,1)S(1)}, u32[]{:S(2)}, u32[]{:S(2)}) %all-to-all-start.2) | async-done | bytes 262176 | tf_op jit(solution)/shard_map/all_to_all | solution.py:136
  232.5 1.3 gather_fusion.1
  233.8 1.5 multiply_reduce_fusion
  235.3 0.7 fusion.25
  (22 shorter events, 0.4 us)
Async XLA Ops:
  6.5 121.7 %copy-start = (bf16[1,256,2048]{2,1,0:T(8,128)(2,1)S(1)}, bf16[1,256,2048]{2,1,0:T(8,128)(2,1)}, u32[]{:S(2)}) copy-start(bf16[1,256,2048]{2,1,0:T(8,128)(2,1)} %param.21) | copy-start | bytes 3145732
  6.5 39.6 %copy-start.5 = (bf16[128]{0:T(256)(128)(2,1)S(1)}, bf16[128]{0:T(256)(128)(2,1)}, u32[]{:S(2)}) copy-start(bf16[128]{0:T(256)(128)(2,1)} %param.16) | copy-start | bytes 772
  7.4 10.3 %collective-permute-start = (bf16[15,64]{0,1:T(8,128)(2,1)S(1)}, bf16[15,64]{0,1:T(8,128)(2,1)S(1)}, u32[]{:S(2)}, u32[]{:S(2)}) collective-permute-start(bf16[15,64]{0,1:T(8,128)(2,1)S(1)} %slice.58), channel_id=1, source_target_pairs={{0,16},{16,32},{32,48},{48,64},{64,80},{80,96},{96,112},{112,128},... | collective-permute-start | bytes 5768 | tf_op jit(solution)/shard_map/ppermute | solution.py:18
  11.6 112.2 %copy-start.3 = (bf16[1,2048,256]{2,1,0:T(8,128)(2,1)S(1)}, bf16[1,2048,256]{2,1,0:T(8,128)(2,1)}, u32[]{:S(2)}) copy-start(bf16[1,2048,256]{2,1,0:T(8,128)(2,1)} %param.19) | copy-start | bytes 3145732
  39.9 10.7 %all-to-all-start = ((f32[16,1,256]{2,1,0:T(1,128)}), f32[16,1,256]{2,1,0:T(1,128)S(1)}, u32[]{:S(2)}, u32[]{:S(2)}) async-start(f32[16,1,256]{2,1,0:T(1,128)} %broadcast_in_dim.187), calls=%async_computation | async-start | bytes 32768 | tf_op jit(solution)/shard_map/all_to_all | solution.py:23
  46.1 77.6 %all-gather.3.cloned.1.call-start = ((), (), s32[]{:S(2)}) async-start(), calls=%async_computation.4 | async-start | bytes 4456448 | tf_op jit(solution)/shard_map/all_gather | solution.py:114
  54.2 74.1 %copy-start.4 = (bf16[1,2048,256]{2,1,0:T(8,128)(2,1)S(1)}, bf16[1,2048,256]{2,1,0:T(8,128)(2,1)}, u32[]{:S(2)}) copy-start(bf16[1,2048,256]{2,1,0:T(8,128)(2,1)} %param.20) | copy-start | bytes 3145732
  78.4 131.2 %reduce-scatter.4.cloned.1.call-start = ((), (), s32[]{:S(2)}) async-start(), calls=%async_computation.5 | async-start | bytes 4456448
  143.5 78.0 %copy-start.1 = (s32[256,2]{0,1:T(2,128)S(1)}, s32[256,2]{0,1:T(2,128)}, u32[]{:S(2)}) copy-start(s32[256,2]{0,1:T(2,128)} %param.17) | copy-start | bytes 6148
  143.5 78.2 %copy-start.2 = (f32[256,2]{0,1:T(2,128)S(1)}, f32[256,2]{0,1:T(2,128)}, u32[]{:S(2)}) copy-start(f32[256,2]{0,1:T(2,128)} %param.18) | copy-start | bytes 6148
  211.4 21.1 %all-to-all-start.2 = ((bf16[128,32,32]{0,2,1:T(8,128)(2,1)}), bf16[128,32,32]{0,2,1:T(8,128)(2,1)S(1)}, u32[]{:S(2)}, u32[]{:S(2)}) async-start(bf16[128,32,32]{0,2,1:T(8,128)(2,1)} %bitcast.14), calls=%async_computation.2 | async-start | bytes 524288 | tf_op jit(solution)/shard_map/all_to_all | solution.py:136
Sparse Core Ops, SparseCore 0:
  78.6 45.1 all-gather.2
  143.7 65.9 reduce-scatter.3
where the time goes:
time: 243 us
  waiting for transfers between devices  126 us (52%)
  blocking collectives  42.1 us (17%)
  starting transfers between devices  19.3 us (8%)
  local copies, waits for them, and re-layouts  19.1 us (8%)
  matrix products  16 us (7%)
  between operations  13.6 us (6%)
  other arithmetic  6.38 us (3%)
    unnamed x3, waiting for transfers between devices  66.1 us
    all_gather x1, waiting for transfers between devices, on_device(): lax.all_gather(lax.all_to_all(sent_rows, 'sp', split_axis=0, concat_axis=...  45.3 us
    all_to_all x1, blocking collectives, on_device(): lax.all_to_all(sent_rows, 'sp', split_axis=0, concat_axis=0, tiled=True)  24.2 us
    all_gather x1, blocking collectives, on_device(): lax.all_gather(mixed_out, 'tp', axis=1, tiled=True)  17.9 us
    all_to_all x1, waiting for transfers between devices, on_device(): lax.all_to_all(result, 'sp', split_axis=1, concat_axis=1, tiled=True)  10.5 us
    all_to_all x1, starting transfers between devices, on_device(): lax.all_to_all(result, 'sp', split_axis=1, concat_axis=1, tiled=True)  9.91 us
    unnamed x16, local copies, waits for them, and re-layouts  9.15 us
    dot_general x1, matrix products, on_device(): lax.dot_general(down_piece, hidden, (((0,), (1,)), ((), ())), preferred_e...  8.85 us
  transfers between devices with their start and end apart: 5, of which 4 were waited for; matrix products, arithmetic and copies ran while one was open for 3% of the time, Pallas kernels for 0%

commit v1 on v0

--- a/solution.py
+++ b/solution.py
@@ -111,11 +111,17 @@
     sent_rows = jnp.take(normed_part, slot_token, axis=0, mode="fill", fill_value=0).reshape(
         experts_all, capacity, features
     )
-    gathered = lax.all_gather(
-        lax.all_to_all(sent_rows, "sp", split_axis=0, concat_axis=0, tiled=True),
-        "tp",
+    gathered = jnp.concatenate(
+        lax.all_to_all(
+            jnp.stack(
+                [lax.all_to_all(sent_rows, "sp", split_axis=0, concat_axis=0, tiled=True)]
+                * lax.axis_size("tp")
+            ),
+            "tp",
+            0,
+            0,
+        ),
         axis=2,
-        tiled=True,
     )
     sources = gathered.shape[0]
     slot_count = gathered.shape[1]

time: 243 us -> 296 us (1.22)
  blocking collectives: 42.1 us -> 143 us
  waiting for transfers between devices: 126 us -> 73.9 us
  local copies, waits for them, and re-layouts: 19.1 us -> 26.7 us
  matrix products: 16 us -> 12.4 us
    all_to_all x0 -> x1, blocking collectives: none -> 101 us  [on_device(): lax.all_to_all(jnp.stack([lax.all_to_all(sent_rows, 'sp', split_axis=0, c...]
    all_gather x1 -> x0, waiting for transfers between devices: 45.3 us -> none  [on_device(): lax.all_gather(lax.all_to_all(sent_rows, 'sp', split_axis=0, concat_axis=...]
    unnamed x3 -> x2, waiting for transfers between devices: 66.1 us -> 59 us
    reshape x0 -> x1, local copies, waits for them, and re-layouts: none -> 4.86 us  [on_device(): jnp.concatenate(lax.all_to_all(jnp.stack([lax.all_to_all(sent_rows, 'sp',...]
    dot_general x1, matrix products: 4.52 us -> 1.25 us  [on_device(): jnp.dot(flattened, expert_gate[0], preferred_element_type=jnp.float32)]
    unnamed x16 -> x18, local copies, waits for them, and re-layouts: 9.15 us -> 11.1 us
  transfers between devices with their start and end apart: 5 -> 4, of which waited for: 4 -> 3; matrix products, arithmetic and copies ran while one was open for 3% -> 3% of each run, Pallas kernels for 0% -> 0%
where the time goes in v1:
time: 296 us; the launch traced here: 295 us
  blocking collectives  143 us (48%)
  waiting for transfers between devices  73.9 us (25%)
  local copies, waits for them, and re-layouts  26.7 us (9%)
  starting transfers between devices  19.2 us (6%)
  between operations  13.7 us (5%)
  matrix products  12.4 us (4%)
  other arithmetic  6.34 us (2%)
    all_to_all x1, blocking collectives, on_device(): lax.all_to_all(jnp.stack([lax.all_to_all(sent_rows, 'sp', split_axis=0, c...  101 us
    unnamed x2, waiting for transfers between devices  59 us
    all_to_all x1, blocking collectives, on_device(): lax.all_to_all(sent_rows, 'sp', split_axis=0, concat_axis=0, tiled=True)  24 us
    all_gather x1, blocking collectives, on_device(): lax.all_gather(mixed_out, 'tp', axis=1, tiled=True)  17.9 us
    unnamed x18, local copies, waits for them, and re-layouts  11.1 us
    all_to_all x1, waiting for transfers between devices, on_device(): lax.all_to_all(result, 'sp', split_axis=1, concat_axis=1, tiled=True)  10.6 us
    all_to_all x1, starting transfers between devices, on_device(): lax.all_to_all(result, 'sp', split_axis=1, concat_axis=1, tiled=True)  9.88 us
    dot_general x1, matrix products, on_device(): lax.dot_general(down_piece, hidden, (((0,), (1,)), ((), ())), preferred_e...  8.53 us
  transfers between devices with their start and end apart: 4, of which 3 were waited for; matrix products, arithmetic and copies ran while one was open for 3% of the time, Pallas kernels for 0%

profile of v1, /device:TPU:25, one launch (start us, length us, event | category | flops | bytes accessed | tf_op | source)
XLA Modules:
  0.0 295.4 jit_solution(8577680851631948550)
XLA Ops:
  6.5 0.0 copy-start
  6.5 0.0 copy-start.6
  6.5 0.9 slice.58
  7.4 3.1 %collective-permute-start = (bf16[15,64]{0,1:T(8,128)(2,1)S(1)}, bf16[15,64]{0,1:T(8,128)(2,1)S(1)}, u32[]{:S(2)}, u32[]{:S(2)}) collective-permute-start(bf16[15,64]{0,1:T(8,128)(2,1)S(1)} %slice.58), channel_id=1, source_target_pairs={{0,16},{16,32},{32,48},{48,64},{64,80},{80,96},{96,112},{112,128},... | collective-permute-start | bytes 5768 | tf_op jit(solution)/shard_map/ppermute | solution.py:18
  10.8 0.8 copy.38
  11.6 0.1 eq.28
  11.7 0.1 reshape.239
  11.9 0.7 broadcast_multiply_fusion
  12.6 1.2 reduce-window.6
  13.7 0.2 slice_reduce_fusion
  14.0 0.1 copy.43
  14.2 0.1 mul.320
  14.3 0.1 reshape.265
  14.5 0.1 fusion.50
  14.6 2.4 scatter_custom_fusion
  17.1 0.7 convert_element_type.62
  17.7 0.0 collective-permute-done
  17.7 0.8 maximum_convert_fusion
  18.6 1.3 fusion.29
  19.9 17.9 %all-gather = bf16[256,1,1024]{0,2,1:T(8,128)(2,1)S(1)} all-gather(bf16[256,1,64]{0,2,1:T(8,128)(2,1)S(1)} %fusion.29), channel_id=2, replica_groups=mesh['sp'=32,'tp'=16] {'tp'}, dimensions={2}, use_global_device_ids=true | all-gather | bytes 557056 | tf_op jit(solution)/shard_map/all_gather | solution.py:97
  37.8 1.3 fusion.26
  39.1 0.1 fusion.44
  39.2 0.6 broadcast_in_dim.187
  39.9 6.2 %all-to-all-start = ((f32[16,1,256]{2,1,0:T(1,128)}), f32[16,1,256]{2,1,0:T(1,128)S(1)}, u32[]{:S(2)}, u32[]{:S(2)}) async-start(f32[16,1,256]{2,1,0:T(1,128)} %broadcast_in_dim.187), calls=%async_computation | async-start | bytes 32768 | tf_op jit(solution)/shard_map/all_to_all | solution.py:23
  46.1 0.0 reduce-scatter.4.cloned.1.call-start
  46.1 0.0 copy-done.6
  46.1 0.1 broadcast_in_dim.185
  46.2 4.4 %all-to-all-done = f32[16,1,256]{2,1,0:T(1,128)S(1)} async-done(((f32[16,1,256]{2,1,0:T(1,128)}), f32[16,1,256]{2,1,0:T(1,128)S(1)}, u32[]{:S(2)}, u32[]{:S(2)}) %all-to-all-start) | async-done | bytes 16416 | tf_op jit(solution)/shard_map/all_to_all | solution.py:23
  50.6 0.1 fusion.46
  50.7 3.2 %gather_fusion = bf16[1024,128]{1,0:T(8,128)(2,1)S(1)} fusion(bf16[256,128]{1,0:T(8,128)(2,1)S(1)} %fusion.46, s32[1024]{0:T(1024)S(1)} %fusion.72), kind=kCustom, calls=%fused_computation | custom fusion | bytes 528384 | tf_op jit(solution)/shard_map/jit(_take)/gather | solution.py:111
  53.9 0.2 broadcast_select_fusion
  54.2 24.0 %all_to_all.21 = bf16[32,32,128]{2,1,0:T(8,128)(2,1)S(1)} all-to-all(bf16[32,32,128]{2,1,0:T(8,128)(2,1)S(1)} %broadcast_select_fusion), channel_id=1, replica_groups=mesh['sp'=32,'tp'=16] {'sp'}, dimensions={0} | all-to-all | bytes 524288 | tf_op jit(solution)/shard_map/all_to_all | solution.py:117
  78.1 0.8 stack.2
  78.9 101.3 %all_to_all.22 = bf16[16,32,32,128]{3,2,1,0:T(8,128)(2,1)S(1)} all-to-all(bf16[16,32,32,128]{3,2,1,0:T(8,128)(2,1)S(1)} %stack.2), channel_id=1, replica_groups=mesh['sp'=32,'tp'=16] {'tp'}, dimensions={0} | all-to-all | bytes 8388608 | tf_op jit(solution)/shard_map/all_to_all | solution.py:115
  180.2 0.0 copy-start.4
  180.2 4.9 %copy.45 = bf16[32,32,16,128]{3,2,1,0:T(8,128)(2,1)S(1)} copy(bf16[32,32,16,128]{3,1,0,2:T(8,128)(2,1)S(1)} %bitcast.83) | data formatting | bytes 8388608 | tf_op jit(solution)/shard_map/reshape | solution.py:114
  185.1 0.0 copy-start.1
  185.1 2.0 copy-done.1
  187.0 0.0 copy-done.4
  187.1 0.0 copy-start.5
  187.1 1.3 fusion.6
  188.3 0.0 copy-done
  188.3 0.0 copy-done.5
  188.3 8.5 %convert_bitcast_fusion = bf16[2048,1024]{0,1:T(8,128)(2,1)} fusion(f32[1024,256]{1,0:T(8,128)S(1)} %fusion.6, bf16[128,8,16,128]{3,2,1,0:T(8,128)(2,1)} %bitcast.86, bf16[1,256,2048]{2,1,0:T(8,128)(2,1)S(1)} %copy-done, bf16[1,2048,256]{2,1,0:T(8,128)(2,1)S(1)} %copy-done.5), kind=kOutput, calls=%fused_computation.7 | convolution fusion | flops 2151940096 | bytes 11534336 | tf_op jit(solution)/shard_map/dot_general | solution.py:134
  196.9 6.4 %copy.47 = bf16[2048,1024]{1,0:T(8,128)(2,1)} copy(bf16[2048,1024]{0,1:T(8,128)(2,1)} %convert_bitcast_fusion) | data formatting | bytes 8388608
  203.3 0.0 copy-start.2
  203.3 0.0 copy-start.3
  203.3 0.0 reduce-scatter.4.cloned.1.call-update
  203.3 59.0 %reduce-scatter.4.cloned.1.call-done = bf16[128,1024]{1,0:T(8,128)(2,1)} async-done(((bf16[2048,1024]{1,0:T(8,128)(2,1)}), bf16[128,1024]{1,0:T(8,128)(2,1)}) %reduce-scatter.4.cloned.1.call-update) | async-done | bytes 262160
  262.3 1.8 copy.48
  264.0 9.9 %all-to-all-start.3 = ((bf16[128,32,32]{0,2,1:T(8,128)(2,1)}), bf16[128,32,32]{0,2,1:T(8,128)(2,1)S(1)}, u32[]{:S(2)}, u32[]{:S(2)}) async-start(bf16[128,32,32]{0,2,1:T(8,128)(2,1)} %bitcast.14), calls=%async_computation.3 | async-start | bytes 524288 | tf_op jit(solution)/shard_map/all_to_all | solution.py:142
  273.9 0.1 reduce_sum.41
  274.1 0.1 copy.41
  274.1 0.0 copy-done.2
  274.2 0.2 copy.42
  274.4 0.0 copy-done.3
  274.4 0.1 copy.46
  274.5 10.6 %all-to-all-done.3 = bf16[128,32,32]{0,2,1:T(8,128)(2,1)S(1)} async-done(((bf16[128,32,32]{0,2,1:T(8,128)(2,1)}), bf16[128,32,32]{0,2,1:T(8,128)(2,1)S(1)}, u32[]{:S(2)}, u32[]{:S(2)}) %all-to-all-start.3) | async-done | bytes 262176 | tf_op jit(solution)/shard_map/all_to_all | solution.py:142
  285.1 1.3 gather_fusion.1
  286.4 1.5 multiply_reduce_fusion
  287.9 0.6 fusion.47
  (22 shorter events, 0.4 us)
Async XLA Ops:
  6.5 181.8 %copy-start = (bf16[1,256,2048]{2,1,0:T(8,128)(2,1)S(1)}, bf16[1,256,2048]{2,1,0:T(8,128)(2,1)}, u32[]{:S(2)}) copy-start(bf16[1,256,2048]{2,1,0:T(8,128)(2,1)} %param.21) | copy-start | bytes 3145732
  6.5 39.6 %copy-start.6 = (bf16[128]{0:T(256)(128)(2,1)S(1)}, bf16[128]{0:T(256)(128)(2,1)}, u32[]{:S(2)}) copy-start(bf16[128]{0:T(256)(128)(2,1)} %param.16) | copy-start | bytes 772
  7.4 10.3 %collective-permute-start = (bf16[15,64]{0,1:T(8,128)(2,1)S(1)}, bf16[15,64]{0,1:T(8,128)(2,1)S(1)}, u32[]{:S(2)}, u32[]{:S(2)}) collective-permute-start(bf16[15,64]{0,1:T(8,128)(2,1)S(1)} %slice.58), channel_id=1, source_target_pairs={{0,16},{16,32},{32,48},{48,64},{64,80},{80,96},{96,112},{112,128},... | collective-permute-start | bytes 5768 | tf_op jit(solution)/shard_map/ppermute | solution.py:18
  39.9 10.7 %all-to-all-start = ((f32[16,1,256]{2,1,0:T(1,128)}), f32[16,1,256]{2,1,0:T(1,128)S(1)}, u32[]{:S(2)}, u32[]{:S(2)}) async-start(f32[16,1,256]{2,1,0:T(1,128)} %broadcast_in_dim.187), calls=%async_computation | async-start | bytes 32768 | tf_op jit(solution)/shard_map/all_to_all | solution.py:23
  46.1 216.2 %reduce-scatter.4.cloned.1.call-start = ((), (), s32[]{:S(2)}) async-start(), calls=%async_computation.5 | async-start | bytes 4456448
  180.2 6.8 %copy-start.4 = (bf16[1,2048,256]{2,1,0:T(8,128)(2,1)S(1)}, bf16[1,2048,256]{2,1,0:T(8,128)(2,1)}, u32[]{:S(2)}) copy-start(bf16[1,2048,256]{2,1,0:T(8,128)(2,1)} %param.19) | copy-start | bytes 3145732
  185.1 2.0 copy-start.1
  187.1 1.3 copy-start.5
  203.3 70.9 %copy-start.2 = (s32[256,2]{0,1:T(2,128)S(1)}, s32[256,2]{0,1:T(2,128)}, u32[]{:S(2)}) copy-start(s32[256,2]{0,1:T(2,128)} %param.17) | copy-start | bytes 6148
  203.3 71.1 %copy-start.3 = (f32[256,2]{0,1:T(2,128)S(1)}, f32[256,2]{0,1:T(2,128)}, u32[]{:S(2)}) copy-start(f32[256,2]{0,1:T(2,128)} %param.18) | copy-start | bytes 6148
  264.0 21.1 %all-to-all-start.3 = ((bf16[128,32,32]{0,2,1:T(8,128)(2,1)}), bf16[128,32,32]{0,2,1:T(8,128)(2,1)S(1)}, u32[]{:S(2)}, u32[]{:S(2)}) async-start(bf16[128,32,32]{0,2,1:T(8,128)(2,1)} %bitcast.14), calls=%async_computation.3 | async-start | bytes 524288 | tf_op jit(solution)/shard_map/all_to_all | solution.py:142
Sparse Core Ops, SparseCore 0:
  203.4 58.7 reduce-scatter.3
